TPU v7x, 512 devices: a whole 4x4x16 slice. The times are simulated.
512 devices in a mesh: sp: 32 (over z, core), tp: 16 (over y, x).
Axes of the slice: x: 4, y: 4, z: 16, core: 2. Of those that a mesh axis runs over, the one named last changes fastest.
Arguments:
- b_gate: bfloat16 [8192, 1024], P('sp', 'tp'), may hold values from -6 to 6
- c_gate: bfloat16 [8192, 1024], P('sp', 'tp'), may hold values from -6 to 6
- h_in: bfloat16 [8192, 1024], P('sp', 'tp'), may hold values from -6 to 6
- docs: int32 [8192], replicated, may hold values from 0 to 15, never falling along the last dimension, each value on 1 to 1024 neighbouring positions
- conv_taps: bfloat16 [3, 1024], replicated, may hold values from -3 to 3
- out_weight: bfloat16 [1024, 4096], P(None, 'tp'), may hold values from -0.1875 to 0.1875
- residual_in: bfloat16 [8192, 4096], P('sp', 'tp'), may hold values from -52 to 52
- norm_gain: bfloat16 [4096], replicated, may hold values from 0.099609375 to 1.8984375
- expert_pick: int32 [8192, 2], P('sp'), may hold values from 0 to 31, as said below
- route_weight: float32 [8192, 2], P('sp'), may hold values from 0.5 to 2
- w_gate: bfloat16 [32, 4096, 2048], P('sp', None, 'tp'), may hold values from -0.09375 to 0.09375
- w_up: bfloat16 [32, 4096, 2048], P('sp', None, 'tp'), may hold values from -0.09375 to 0.09375
- w_down: bfloat16 [32, 2048, 4096], P('sp', None, 'tp'), may hold values from -0.125 to 0.125
Outputs:
- stream_out: bfloat16 [8192, 4096], P('sp', 'tp')
Inputs may be any that keep to these rules, and one draw needn't show every extreme that they name: `expert_pick`: each row names 2 different experts of one group; group g holds experts g * 8 up to the next group's first.
All inputs are finite; a program needn't handle non-finite values.
Results may differ from a plain program's by a relative error of at most 0.012.
Values may be sent and summed in bfloat16 or wider, within the bound.
No kernel may reach another device: no remote copies, remote signals or barrier semaphores. Data moves between devices by JAX's collectives and lax.ppermute only.
A program may use at most 64 MiB of HBM per device.

v0:
```python
import jax
import jax.numpy as jnp
from jax import lax
from jax.sharding import Mesh
from jax.sharding import PartitionSpec as P

TOP_K = 2
TP = ("tp_0", "tp_1")
NORM_EPS = 1e-06


def passed_along(value, axis, steps):
    count = lax.axis_size(axis)
    first, last = (max(0, -steps), min(count, count - steps))
    return lax.ppermute(value, axis, [(source, source + steps) for source in range(first, last)])


def laid_out(tiles, dim):
    shape = list(tiles.shape[1:])
    shape[dim] *= tiles.shape[0]
    return jnp.moveaxis(tiles, 0, dim).reshape(shape)


def from_everyone(shard, axis):
    devices = lax.axis_size(axis)
    return lax.all_to_all(
        jnp.broadcast_to(shard[None], (devices, *shard.shape)), axis, 0, 0, tiled=True
    )


def collect(shard, axis, dim):
    return laid_out(from_everyone(shard, axis), dim)


def by_axis(shard, axes):
    for axis in axes:
        shard = lax.psum(shard, axis)
    return shard


def local(
    b_gate,
    c_gate,
    h_in,
    docs,
    conv_taps,
    out_weight,
    residual_in,
    norm_gain,
    expert_pick,
    route_weight,
    w_gate,
    w_up,
    w_down,
):
    tok_rows, local_chans = h_in.shape
    width = residual_in.shape[1]
    full_dim = w_gate.shape[1]
    n_sp = lax.axis_size("sp")
    sp_index = lax.axis_index("sp")
    tp_index = lax.axis_index(TP)
    first_pos = sp_index * tok_rows
    product = (c_gate.astype(jnp.float32) * h_in.astype(jnp.float32)).astype(jnp.bfloat16)
    edge = passed_along(product[tok_rows - 2 :], "sp", 1)
    extended = jnp.concatenate([edge, product], axis=0).astype(jnp.float32)
    own_docs = lax.dynamic_slice_in_dim(docs, first_pos, tok_rows)
    padded_docs = jnp.concatenate([jnp.full((2,), -1, jnp.int32), docs], axis=0)
    near_docs = lax.dynamic_slice_in_dim(padded_docs, first_pos, tok_rows + 2)
    tap_weights = lax.dynamic_slice_in_dim(
        conv_taps, tp_index * local_chans, local_chans, 1
    ).astype(jnp.float32)
    conv_sum = tap_weights[0][None, :] * extended[2:]
    for step_back in (1, 2):
        same_doc = (near_docs[2 - step_back : 2 - step_back + tok_rows] == own_docs).astype(
            jnp.float32
        )[:, None]
        conv_sum = (
            conv_sum
            + tap_weights[step_back][None, :]
            * extended[2 - step_back : 2 - step_back + tok_rows]
            * same_doc
        )
    conv_out = (b_gate.astype(jnp.float32) * conv_sum).astype(jnp.bfloat16)
    projected = jnp.dot(collect(conv_out, TP, 1), out_weight, preferred_element_type=jnp.float32)
    stream = (residual_in.astype(jnp.float32) + projected).astype(jnp.bfloat16)
    stream_f = stream.astype(jnp.float32)
    capacity = 5 * tok_rows // (2 * n_sp)
    assign_flat = expert_pick.reshape(-1)
    onehot = (assign_flat[:, None] == jnp.arange(n_sp, dtype=jnp.int32)[None, :]).astype(jnp.int32)
    slot_pos = jnp.sum((jnp.cumsum(onehot, axis=0) - onehot) * onehot, axis=1)
    kept_mask = slot_pos < capacity
    target = jnp.where(
        kept_mask, assign_flat * capacity + jnp.minimum(slot_pos, capacity - 1), n_sp * capacity
    )
    table = (
        jnp.full((n_sp * capacity + 1,), -1, jnp.int32)
        .at[target]
        .set(jnp.arange(assign_flat.shape[0], dtype=jnp.int32))[:-1]
    )
    filled = table >= 0
    source_rows = jnp.maximum(table, 0) // TOP_K
    gate_local = w_gate[0]
    up_local = w_up[0]
    slot_rows = n_sp * capacity
    squares = by_axis(jnp.sum(stream_f * stream_f, axis=1), TP)
    inverse = lax.rsqrt(squares / full_dim + NORM_EPS)[:, None]
    gain_cols = lax.dynamic_slice_in_dim(norm_gain, tp_index * width, width).astype(jnp.float32)
    normed = (stream_f * inverse * gain_cols[None, :]).astype(jnp.bfloat16)
    outgoing = jnp.where(filled[:, None], normed[source_rows], jnp.zeros((), normed.dtype)).reshape(
        n_sp, capacity, width
    )
    received = lax.all_to_all(outgoing, "sp", split_axis=0, concat_axis=0, tiled=True)
    shard_piece = lax.all_gather(received, TP, axis=2, tiled=True)
    flat_piece = shard_piece.reshape(slot_rows, shard_piece.shape[2])
    gate_pre = jnp.dot(flat_piece, gate_local, preferred_element_type=jnp.float32)
    up_pre = jnp.dot(flat_piece, up_local, preferred_element_type=jnp.float32)
    hidden = (jax.nn.silu(gate_pre) * up_pre).astype(jnp.bfloat16)
    down_local = w_down[0]
    result = jnp.dot(collect(hidden, TP, 1), down_local, preferred_element_type=jnp.float32).astype(
        jnp.bfloat16
    )
    returned = lax.all_to_all(
        result.reshape(n_sp, capacity, width), "sp", split_axis=0, concat_axis=0, tiled=True
    ).reshape(n_sp * capacity, width)
    picked = jnp.where(
        kept_mask[:, None],
        returned[jnp.minimum(target, n_sp * capacity - 1)].astype(jnp.float32),
        0.0,
    )
    weighted = picked * route_weight.reshape(-1)[:, None]
    feed_out = jnp.sum(weighted.reshape(tok_rows, TOP_K, width), axis=1)
    return (stream_f + feed_out).astype(jnp.bfloat16)


def solution(mesh):
    finer = Mesh(mesh.devices.reshape(mesh.shape["sp"], 4, 4), ("sp", "tp_0", "tp_1"))
    placed = (
        P("sp", TP),
        P("sp", TP),
        P("sp", TP),
        P(),
        P(),
        P(None, TP),
        P("sp", TP),
        P(),
        P("sp", None),
        P("sp", None),
        P("sp", None, TP),
        P("sp", None, TP),
        P("sp", None, TP),
    )
    return jax.shard_map(local, mesh=finer, in_specs=placed, out_specs=P("sp", TP), check_vma=False)
```

profile of v0, /device:TPU:1, one launch (start us, length us, event | category | flops | bytes accessed | tf_op | source)
XLA Modules:
  0.0 282.6 jit_solution(15302591660513541208)
XLA Ops:
  6.5 0.9 multiply_convert_fusion.1
  7.5 4.9 %collective-permute-start = (bf16[2,64]{0,1:T(8,128)(2,1)S(1)}, bf16[2,64]{0,1:T(8,128)(2,1)S(1)}, u32[]{:S(2)}, u32[]{:S(2)}) collective-permute-start(bf16[2,64]{0,1:T(8,128)(2,1)S(1)} %slice.52), channel_id=1, source_target_pairs={{0,16},{16,32},{32,48},{48,64},{64,80},{80,96},{96,112},{112,128},... | collective-permute-start | bytes 776 | tf_op jit(solution)/shard_map/ppermute | solution.py:15
  12.4 0.8 copy.29
  13.2 0.1 eq.37
  13.4 0.1 eq.33
  13.5 1.2 reduce-window.6
  14.7 0.2 slice_reduce_fusion
  15.0 0.1 fusion.9
  15.1 0.7 broadcast_multiply_fusion
  15.8 0.7 dynamic-slice_convert_fusion
  16.5 0.1 copy.32
  16.7 0.1 mul.139
  16.8 0.8 pad_dynamic-slice_fusion
  17.6 0.8 compare_convert_fusion.1
  18.4 2.4 scatter_custom_fusion
  21.0 0.9 fusion.13
  21.9 0.8 broadcast_in_dim.32
  22.7 6.8 %all-to-all-start = ((bf16[16,256,64]{1,2,0:T(8,128)(2,1)}), bf16[16,256,64]{1,2,0:T(8,128)(2,1)S(1)}, u32[]{:S(2)}, u32[]{:S(2)}) async-start(bf16[16,256,64]{1,2,0:T(8,128)(2,1)} %broadcast_in_dim.32), calls=%async_computation | async-start | bytes 1048576 | tf_op jit(solution)/shard_map/all_to_all | solution.py:26
  29.5 1.0 copy.28
  30.5 0.1 ge.8
  30.7 0.8 dynamic-slice_convert_fusion.1
  31.4 9.4 %all-to-all-done = bf16[16,256,64]{1,2,0:T(8,128)(2,1)S(1)} async-done(((bf16[16,256,64]{1,2,0:T(8,128)(2,1)}), bf16[16,256,64]{1,2,0:T(8,128)(2,1)S(1)}, u32[]{:S(2)}, u32[]{:S(2)}) %all-to-all-start) | async-done | bytes 524320 | tf_op jit(solution)/shard_map/all_to_all | solution.py:26
  40.8 1.4 multiply_reduce_fusion.1
  42.2 6.9 %psum.14 = f32[256]{0:T(256)S(1)} all-reduce(f32[256]{0:T(256)S(1)} %get-tuple-element.12), channel_id=1, replica_groups=mesh['sp'=32,'tp_0'=4,'tp_1'=4] {'tp_0'}, use_global_device_ids=true, to_apply=%region_5.6 | all-reduce | flops 256 | bytes 2048 | tf_op jit(solution)/shard_map/psum | solution.py:37
  49.1 6.3 %psum.15 = f32[256]{0:T(256)S(1)} all-reduce(f32[256]{0:T(256)S(1)} %psum.14), channel_id=1, replica_groups=mesh['sp'=32,'tp_0'=4,'tp_1'=4] {'tp_1'}, use_global_device_ids=true, to_apply=%region_6.7 | all-reduce | flops 256 | bytes 2048 | tf_op jit(solution)/shard_map/psum | solution.py:37
  55.4 0.1 multiply_convert_fusion
  55.6 2.8 gather_fusion
  58.5 0.2 broadcast_select_fusion
  58.7 47.2 %all_to_all.20 = bf16[32,20,256]{2,1,0:T(8,128)(2,1)} all-to-all(bf16[32,20,256]{2,1,0:T(8,128)(2,1)S(1)} %broadcast_select_fusion), channel_id=1, replica_groups=mesh['sp'=32,'tp_0'=4,'tp_1'=4] {'sp'}, dimensions={0} | all-to-all | bytes 655360 | tf_op jit(solution)/shard_map/all_to_all | solution.py:112
  105.9 68.7 %all-gather.2.cloned.1.call-done = bf16[32,20,4096]{2,1,0:T(8,128)(2,1)} async-done(((bf16[32,20,256]{2,1,0:T(8,128)(2,1)}), bf16[32,20,4096]{2,1,0:T(8,128)(2,1)}) %all-gather.2.cloned.1.call-update) | async-done | bytes 5242896 | tf_op jit(solution)/shard_map/all_gather | solution.py:113
  174.6 7.8 %reshape.133 = bf16[640,4096]{1,0:T(8,128)(2,1)} reshape(bf16[32,20,4096]{2,1,0:T(8,128)(2,1)} %all-gather.2.cloned.1.call-done) | data formatting | bytes 10485760 | tf_op jit(solution)/shard_map/reshape | solution.py:114
  182.5 4.1 %fusion.5 = f32[640,128]{1,0:T(8,128)S(1)} fusion(bf16[640,4096]{1,0:T(8,128)(2,1)} %reshape.133, bf16[1,4096,128]{2,1,0:T(8,128)(2,1)S(1)} %copy-done.3), kind=kOutput, calls=%fused_computation.11 | convolution fusion | flops 671088640 | bytes 6619136 | tf_op jit(solution)/shard_map/dot_general | solution.py:115
  186.7 0.2 copy-done.4
  186.8 1.5 fusion
  188.3 0.2 copy.34
  188.5 0.3 broadcast_in_dim.62
  188.8 37.3 %all_to_all.21 = bf16[16,640,128]{1,2,0:T(8,128)(2,1)S(1)} all-to-all(bf16[16,640,128]{1,2,0:T(8,128)(2,1)S(1)} %broadcast_in_dim.62), channel_id=1, replica_groups=mesh['sp'=32,'tp_0'=4,'tp_1'=4] {'tp_0','tp_1'}, dimensions={0} | all-to-all | bytes 5242880 | tf_op jit(solution)/shard_map/all_to_all | solution.py:26
  226.2 0.9 convolution_convert_fusion
  227.1 0.8 reshape.135
  227.9 15.4 %all-to-all-start.3 = ((bf16[32,20,256]{2,1,0:T(8,128)(2,1)}), bf16[32,20,256]{2,1,0:T(8,128)(2,1)S(1)}, u32[]{:S(2)}, u32[]{:S(2)}) async-start(bf16[32,20,256]{2,1,0:T(8,128)(2,1)} %reshape.135), calls=%async_computation.3 | async-start | bytes 786432 | tf_op jit(solution)/shard_map/all_to_all | solution.py:122
  243.3 0.2 lt.59
  243.5 0.1 copy.35
  243.6 27.4 %all-to-all-done.3 = bf16[32,20,256]{2,1,0:T(8,128)(2,1)S(1)} async-done(((bf16[32,20,256]{2,1,0:T(8,128)(2,1)}), bf16[32,20,256]{2,1,0:T(8,128)(2,1)S(1)}, u32[]{:S(2)}, u32[]{:S(2)}) %all-to-all-start.3) | async-done | bytes 327712 | tf_op jit(solution)/shard_map/all_to_all | solution.py:122
  271.1 2.0 gather_fusion.1
  273.1 0.3 reshape.137
  273.4 1.5 multiply_reduce_fusion
  274.9 0.1 copy.36
  275.0 0.8 copy.37
  (31 shorter events, 0.6 us)
Async XLA Ops:
  6.5 219.6 %copy-start = (bf16[1,2048,256]{2,1,0:T(8,128)(2,1)S(1)}, bf16[1,2048,256]{2,1,0:T(8,128)(2,1)}, u32[]{:S(2)}) copy-start(bf16[1,2048,256]{2,1,0:T(8,128)(2,1)} %param.25) | copy-start | bytes 3145732
  7.5 13.4 %collective-permute-start = (bf16[2,64]{0,1:T(8,128)(2,1)S(1)}, bf16[2,64]{0,1:T(8,128)(2,1)S(1)}, u32[]{:S(2)}, u32[]{:S(2)}) collective-permute-start(bf16[2,64]{0,1:T(8,128)(2,1)S(1)} %slice.52), channel_id=1, source_target_pairs={{0,16},{16,32},{32,48},{48,64},{64,80},{80,96},{96,112},{112,128},... | collective-permute-start | bytes 776 | tf_op jit(solution)/shard_map/ppermute | solution.py:15
  22.7 18.1 %all-to-all-start = ((bf16[16,256,64]{1,2,0:T(8,128)(2,1)}), bf16[16,256,64]{1,2,0:T(8,128)(2,1)S(1)}, u32[]{:S(2)}, u32[]{:S(2)}) async-start(bf16[16,256,64]{1,2,0:T(8,128)(2,1)} %broadcast_in_dim.32), calls=%async_computation | async-start | bytes 1048576 | tf_op jit(solution)/shard_map/all_to_all | solution.py:26
  29.5 145.2 %all-gather.2.cloned.1.call-start = ((), (), s32[]{:S(2)}) async-start(), calls=%async_computation.4 | async-start | bytes 6684672 | tf_op jit(solution)/shard_map/all_gather | solution.py:113
  105.9 76.5 %copy-start.3 = (bf16[1,4096,128]{2,1,0:T(8,128)(2,1)S(1)}, bf16[1,4096,128]{2,1,0:T(8,128)(2,1)}, u32[]{:S(2)}) copy-start(bf16[1,4096,128]{2,1,0:T(8,128)(2,1)} %param.23) | copy-start | bytes 3145732
  182.5 4.2 %copy-start.1 = (bf16[640,4096]{1,0:T(8,128)(2,1)S(1)}, bf16[640,4096]{1,0:T(8,128)(2,1)}, u32[]{:S(2)}) copy-start(bf16[640,4096]{1,0:T(8,128)(2,1)} %reshape.133) | copy-start | bytes 15728644
  182.5 4.3 %copy-start.4 = (bf16[1,4096,128]{2,1,0:T(8,128)(2,1)S(1)}, bf16[1,4096,128]{2,1,0:T(8,128)(2,1)}, u32[]{:S(2)}) copy-start(bf16[1,4096,128]{2,1,0:T(8,128)(2,1)} %param.24) | copy-start | bytes 3145732
  226.2 17.3 %copy-start.2 = (f32[256,2]{0,1:T(2,128)S(1)}, f32[256,2]{0,1:T(2,128)}, u32[]{:S(2)}) copy-start(f32[256,2]{0,1:T(2,128)} %param.22) | copy-start | bytes 6148
  227.9 43.2 %all-to-all-start.3 = ((bf16[32,20,256]{2,1,0:T(8,128)(2,1)}), bf16[32,20,256]{2,1,0:T(8,128)(2,1)S(1)}, u32[]{:S(2)}, u32[]{:S(2)}) async-start(bf16[32,20,256]{2,1,0:T(8,128)(2,1)} %reshape.135), calls=%async_computation.3 | async-start | bytes 786432 | tf_op jit(solution)/shard_map/all_to_all | solution.py:122
Sparse Core Ops, SparseCore 0:
  106.1 68.5 all-gather.1
where the time goes:
time: 284 us; the launch traced here: 283 us
  waiting for transfers between devices  106 us (37%)
  blocking collectives  97.8 us (34%)
  starting transfers between devices  27.1 us (10%)
  local copies, waits for them, and re-layouts  22.6 us (8%)
  between operations  13.7 us (5%)
  other arithmetic  7.98 us (3%)
  matrix products  7.96 us (3%)
    all_gather x1, waiting for transfers between devices, local(): shard_piece = lax.all_gather(received, TP, axis=2, tiled=True)  68.7 us
    all_to_all x1, blocking collectives, local(): lax.all_to_all(outgoing, 'sp', split_axis=0, concat_axis=0, tiled=True)  47.2 us
    all_to_all x1, blocking collectives, from_everyone(): lax.all_to_all(jnp.broadcast_to(shard[None], (devices, *shard.shape)), ax...  37.3 us
    all_to_all x1, waiting for transfers between devices, local(): lax.all_to_all(result.reshape(n_sp, capacity, width), 'sp', split_axis=0,...  27.4 us
    all_to_all x1, starting transfers between devices, local(): lax.all_to_all(result.reshape(n_sp, capacity, width), 'sp', split_axis=0,...  15.4 us
    psum x2, blocking collectives, by_axis(): shard = lax.psum(shard, axis)  13.2 us
    all_to_all x1, waiting for transfers between devices, from_everyone(): lax.all_to_all(jnp.broadcast_to(shard[None], (devices, *shard.shape)), ax...  9.4 us
    reshape x1, local copies, waits for them, and re-layouts, local(): flat_piece = shard_piece.reshape(slot_rows, shard_piece.shape[2])  7.84 us
  transfers between devices with their start and end apart: 4, of which 3 were waited for; matrix products, arithmetic and copies ran while one was open for 4% of the time, Pallas kernels for 0%

commit v1 on v0

--- a/solution.py
+++ b/solution.py
@@ -7,6 +7,19 @@
 TOP_K = 2
 TP = ("tp_0", "tp_1")
 NORM_EPS = 1e-06
+
+
+def _take_table(s0, device_axis):
+    wide_out = jnp.concatenate(
+        jax.lax.all_to_all(
+            jnp.stack([s0 for _ in range(jax.lax.axis_size(device_axis))], axis=0),
+            device_axis,
+            0,
+            0,
+        ),
+        2,
+    )
+    return wide_out
 
 
 def passed_along(value, axis, steps):
@@ -110,7 +123,7 @@
         n_sp, capacity, width
     )
     received = lax.all_to_all(outgoing, "sp", split_axis=0, concat_axis=0, tiled=True)
-    shard_piece = lax.all_gather(received, TP, axis=2, tiled=True)
+    shard_piece = _take_table(received, TP)
     flat_piece = shard_piece.reshape(slot_rows, shard_piece.shape[2])
     gate_pre = jnp.dot(flat_piece, gate_local, preferred_element_type=jnp.float32)
     up_pre = jnp.dot(flat_piece, up_local, preferred_element_type=jnp.float32)

time: 284 us -> 251 us (0.88)
  waiting for transfers between devices: 106 us -> 36.9 us
  blocking collectives: 97.8 us -> 160 us
  between operations: 13.7 us -> 0.34 us
  starting transfers between devices: 27.1 us -> 18.2 us
    all_gather x1 -> x0, waiting for transfers between devices: 68.7 us -> none  [local(): shard_piece = lax.all_gather(received, TP, axis=2, tiled=True)]
    all_to_all x0 -> x1, blocking collectives: none -> 63.8 us  [_take_table(): jax.lax.all_to_all(jnp.stack([s0 for _ in range(jax.lax.axis_size(device_...]
    all_to_all x1, starting transfers between devices: 15.4 us -> 6.57 us  [local(): lax.all_to_all(result.reshape(n_sp, capacity, width), 'sp', split_axis=0,...]
    reshape x1, local copies, waits for them, and re-layouts: 7.84 us -> 2.97 us  [_take_table(): jnp.concatenate(jax.lax.all_to_all(jnp.stack([s0 for _ in range(jax.lax.a...]
    unnamed x13 -> x12, local copies, waits for them, and re-layouts: 2.13 us -> 5.48 us
  transfers between devices with their start and end apart: 4 -> 3, of which waited for: 3 -> 2; matrix products, arithmetic and copies ran while one was open for 4% -> 4% of each run, Pallas kernels for 0% -> 0%
where the time goes in v1:
time: 251 us
  blocking collectives  160 us (64%)
  waiting for transfers between devices  36.9 us (15%)
  local copies, waits for them, and re-layouts  21.8 us (9%)
  starting transfers between devices  18.2 us (7%)
  other arithmetic  7.98 us (3%)
  matrix products  5.31 us (2%)
    all_to_all x1, blocking collectives, _take_table(): jax.lax.all_to_all(jnp.stack([s0 for _ in range(jax.lax.axis_size(device_...  63.8 us
    all_to_all x1, blocking collectives, local(): lax.all_to_all(outgoing, 'sp', split_axis=0, concat_axis=0, tiled=True)  47.1 us
    all_to_all x1, blocking collectives, from_everyone(): lax.all_to_all(jnp.broadcast_to(shard[None], (devices, *shard.shape)), ax...  36 us
    all_to_all x1, waiting for transfers between devices, local(): lax.all_to_all(result.reshape(n_sp, capacity, width), 'sp', split_axis=0,...  27.4 us
    psum x2, blocking collectives, by_axis(): shard = lax.psum(shard, axis)  13.2 us
    all_to_all x1, waiting for transfers between devices, from_everyone(): lax.all_to_all(jnp.broadcast_to(shard[None], (devices, *shard.shape)), ax...  9.45 us
    all_to_all x1, starting transfers between devices, from_everyone(): lax.all_to_all(jnp.broadcast_to(shard[None], (devices, *shard.shape)), ax...  6.75 us
    all_to_all x1, starting transfers between devices, local(): lax.all_to_all(result.reshape(n_sp, capacity, width), 'sp', split_axis=0,...  6.57 us
  transfers between devices with their start and end apart: 3, of which 2 were waited for; matrix products, arithmetic and copies ran while one was open for 4% of the time, Pallas kernels for 0%

profile of v1, /device:TPU:1, one launch (start us, length us, event | category | flops | bytes accessed | tf_op | source)
XLA Modules:
  0.0 250.6 jit_solution(14769073404117762079)
XLA Ops:
  0.0 0.9 multiply_convert_fusion.1
  1.0 4.9 %collective-permute-start = (bf16[2,64]{0,1:T(8,128)(2,1)S(1)}, bf16[2,64]{0,1:T(8,128)(2,1)S(1)}, u32[]{:S(2)}, u32[]{:S(2)}) collective-permute-start(bf16[2,64]{0,1:T(8,128)(2,1)S(1)} %slice.52), channel_id=1, source_target_pairs={{0,16},{16,32},{32,48},{48,64},{64,80},{80,96},{96,112},{112,128},... | collective-permute-start | bytes 776 | tf_op jit(solution)/shard_map/ppermute | solution.py:28
  5.9 0.8 copy.40
  6.7 0.1 eq.37
  6.8 0.1 eq.33
  7.0 1.2 reduce-window.6
  8.2 0.2 slice_reduce_fusion
  8.4 0.1 fusion.9
  8.6 0.7 broadcast_multiply_fusion
  9.3 0.7 dynamic-slice_convert_fusion
  10.0 0.1 copy.43
  10.2 0.1 mul.139
  10.3 0.8 pad_dynamic-slice_fusion
  11.1 0.8 compare_convert_fusion.1
  11.9 2.4 scatter_custom_fusion
  14.4 0.9 fusion.13
  15.3 0.8 broadcast_in_dim.32
  16.2 6.8 %all-to-all-start = ((bf16[16,256,64]{1,2,0:T(8,128)(2,1)}), bf16[16,256,64]{1,2,0:T(8,128)(2,1)S(1)}, u32[]{:S(2)}, u32[]{:S(2)}) async-start(bf16[16,256,64]{1,2,0:T(8,128)(2,1)} %broadcast_in_dim.32), calls=%async_computation | async-start | bytes 1048576 | tf_op jit(solution)/shard_map/all_to_all | solution.py:39
  22.9 1.0 copy.39
  24.0 0.1 ge.8
  24.1 0.8 dynamic-slice_convert_fusion.1
  24.8 9.4 %all-to-all-done = bf16[16,256,64]{1,2,0:T(8,128)(2,1)S(1)} async-done(((bf16[16,256,64]{1,2,0:T(8,128)(2,1)}), bf16[16,256,64]{1,2,0:T(8,128)(2,1)S(1)}, u32[]{:S(2)}, u32[]{:S(2)}) %all-to-all-start) | async-done | bytes 524320 | tf_op jit(solution)/shard_map/all_to_all | solution.py:39
  34.3 1.4 multiply_reduce_fusion.1
  35.7 6.9 %psum.14 = f32[256]{0:T(256)S(1)} all-reduce(f32[256]{0:T(256)S(1)} %get-tuple-element.12), channel_id=1, replica_groups=mesh['sp'=32,'tp_0'=4,'tp_1'=4] {'tp_0'}, use_global_device_ids=true, to_apply=%region_5.6 | all-reduce | flops 256 | bytes 2048 | tf_op jit(solution)/shard_map/psum | solution.py:50
  42.6 6.3 %psum.15 = f32[256]{0:T(256)S(1)} all-reduce(f32[256]{0:T(256)S(1)} %psum.14), channel_id=1, replica_groups=mesh['sp'=32,'tp_0'=4,'tp_1'=4] {'tp_1'}, use_global_device_ids=true, to_apply=%region_6.7 | all-reduce | flops 256 | bytes 2048 | tf_op jit(solution)/shard_map/psum | solution.py:50
  49.1 2.8 %gather_fusion = bf16[640,256]{1,0:T(8,128)(2,1)S(1)} fusion(bf16[256,256]{1,0:T(8,128)(2,1)S(1)} %copy.44, s32[1024]{0:T(1024)S(1)} %pad_clamp_fusion.1), kind=kCustom, calls=%fused_computation | custom fusion | bytes 657920 | tf_op jit(solution)/shard_map/gather | solution.py:122
  52.0 0.2 broadcast_select_fusion
  52.1 47.1 %all_to_all.25 = bf16[32,20,256]{2,1,0:T(8,128)(2,1)S(1)} all-to-all(bf16[32,20,256]{2,1,0:T(8,128)(2,1)S(1)} %broadcast_select_fusion), channel_id=1, replica_groups=mesh['sp'=32,'tp_0'=4,'tp_1'=4] {'sp'}, dimensions={0} | all-to-all | bytes 655360 | tf_op jit(solution)/shard_map/all_to_all | solution.py:125
  99.3 0.7 stack.2
  100.0 63.8 %all_to_all.26 = bf16[16,32,20,256]{3,1,2,0:T(8,128)(2,1)S(1)} all-to-all(bf16[16,32,20,256]{3,1,2,0:T(8,128)(2,1)S(1)} %stack.2), channel_id=1, replica_groups=mesh['sp'=32,'tp_0'=4,'tp_1'=4] {'tp_0','tp_1'}, dimensions={0} | all-to-all | bytes 10485760 | tf_op jit(solution)/shard_map/all_to_all | solution.py:14
  163.8 3.0 %copy.46 = bf16[32,20,16,256]{3,2,1,0:T(8,128)(2,1)S(1)} copy(bf16[32,20,16,256]{3,0,1,2:T(8,128)(2,1)S(1)} %bitcast.52) | data formatting | bytes 10485760 | tf_op jit(solution)/shard_map/reshape | solution.py:13
  166.8 3.5 %copy.52 = bf16[80,8,16,256]{3,1,2,0:T(8,128)(2,1)S(1)} copy(bf16[80,8,16,256]{3,2,1,0:T(8,128)(2,1)S(1)} %bitcast.53) | data formatting | bytes 10485760
  170.3 1.5 fusion.5
  171.9 1.5 fusion
  173.4 0.2 copy.47
  173.5 0.3 broadcast_in_dim.62
  173.8 36.0 %all_to_all.27 = bf16[16,640,128]{1,2,0:T(8,128)(2,1)S(1)} all-to-all(bf16[16,640,128]{1,2,0:T(8,128)(2,1)S(1)} %broadcast_in_dim.62), channel_id=1, replica_groups=mesh['sp'=32,'tp_0'=4,'tp_1'=4] {'tp_0','tp_1'}, dimensions={0} | all-to-all | bytes 5242880 | tf_op jit(solution)/shard_map/all_to_all | solution.py:39
  209.8 0.9 convolution_convert_fusion
  210.7 0.8 reshape.137
  211.5 6.6 %all-to-all-start.4 = ((bf16[32,20,256]{2,1,0:T(8,128)(2,1)}), bf16[32,20,256]{2,1,0:T(8,128)(2,1)S(1)}, u32[]{:S(2)}, u32[]{:S(2)}) async-start(bf16[32,20,256]{2,1,0:T(8,128)(2,1)} %reshape.137), calls=%async_computation.4 | async-start | bytes 786432 | tf_op jit(solution)/shard_map/all_to_all | solution.py:135
  218.1 0.2 lt.59
  218.3 0.1 copy.48
  218.4 27.4 %all-to-all-done.4 = bf16[32,20,256]{2,1,0:T(8,128)(2,1)S(1)} async-done(((bf16[32,20,256]{2,1,0:T(8,128)(2,1)}), bf16[32,20,256]{2,1,0:T(8,128)(2,1)S(1)}, u32[]{:S(2)}, u32[]{:S(2)}) %all-to-all-start.4) | async-done | bytes 327712 | tf_op jit(solution)/shard_map/all_to_all | solution.py:135
  245.9 2.0 gather_fusion.1
  247.9 0.3 reshape.139
  248.2 1.5 multiply_reduce_fusion
  249.7 0.1 copy.49
  249.8 0.8 copy.50
  (30 shorter events, 0.7 us)
Async XLA Ops:
  0.0 209.8 %copy-start = (bf16[1,2048,256]{2,1,0:T(8,128)(2,1)S(1)}, bf16[1,2048,256]{2,1,0:T(8,128)(2,1)}, u32[]{:S(2)}) copy-start(bf16[1,2048,256]{2,1,0:T(8,128)(2,1)} %param.25) | copy-start | bytes 3145732
  1.0 13.4 %collective-permute-start = (bf16[2,64]{0,1:T(8,128)(2,1)S(1)}, bf16[2,64]{0,1:T(8,128)(2,1)S(1)}, u32[]{:S(2)}, u32[]{:S(2)}) collective-permute-start(bf16[2,64]{0,1:T(8,128)(2,1)S(1)} %slice.52), channel_id=1, source_target_pairs={{0,16},{16,32},{32,48},{48,64},{64,80},{80,96},{96,112},{112,128},... | collective-permute-start | bytes 776 | tf_op jit(solution)/shard_map/ppermute | solution.py:28
  16.2 18.1 %all-to-all-start = ((bf16[16,256,64]{1,2,0:T(8,128)(2,1)}), bf16[16,256,64]{1,2,0:T(8,128)(2,1)S(1)}, u32[]{:S(2)}, u32[]{:S(2)}) async-start(bf16[16,256,64]{1,2,0:T(8,128)(2,1)} %broadcast_in_dim.32), calls=%async_computation | async-start | bytes 1048576 | tf_op jit(solution)/shard_map/all_to_all | solution.py:39
  166.8 3.5 %copy-start.2 = (bf16[1,4096,128]{2,1,0:T(8,128)(2,1)S(1)}, bf16[1,4096,128]{2,1,0:T(8,128)(2,1)}, u32[]{:S(2)}) copy-start(bf16[1,4096,128]{2,1,0:T(8,128)(2,1)} %param.23) | copy-start | bytes 3145732
  170.3 1.5 copy-start.3
  209.8 8.5 %copy-start.1 = (f32[256,2]{0,1:T(2,128)S(1)}, f32[256,2]{0,1:T(2,128)}, u32[]{:S(2)}) copy-start(f32[256,2]{0,1:T(2,128)} %param.22) | copy-start | bytes 6148
  211.5 34.3 %all-to-all-start.4 = ((bf16[32,20,256]{2,1,0:T(8,128)(2,1)}), bf16[32,20,256]{2,1,0:T(8,128)(2,1)S(1)}, u32[]{:S(2)}, u32[]{:S(2)}) async-start(bf16[32,20,256]{2,1,0:T(8,128)(2,1)} %reshape.137), calls=%async_computation.4 | async-start | bytes 786432 | tf_op jit(solution)/shard_map/all_to_all | solution.py:135
